TPU v7x, 32 devices: a whole 2x2x4 slice. The times are simulated.
32 devices in a mesh: fs: 16 (over z, y, x), tp: 2 (over core).
Axes of the slice: x: 2, y: 2, z: 4, core: 2. Of those that a mesh axis runs over, the one named last changes fastest.
Arguments:
- residual_in: bfloat16 [4096, 2048], P(('fs', 'tp')), may hold values from -6 to 6
- gain_first: float32 [2048], replicated, may hold values from 0.1 to 1.9
- gain_mixer: float32 [2048], replicated, may hold values from 0.1 to 1.9
- gain_second: float32 [2048], replicated, may hold values from 0.1 to 1.9
- gate_weight: float32 [2048, 6144], P('fs', 'tp'), may hold values from -0.125 to 0.125
- gate_scale: float32 [6144], P('tp'), may hold values from 0.3 to 3
- up_weight: float32 [2048, 6144], P('fs', 'tp'), may hold values from -0.125 to 0.125
- up_scale: float32 [6144], P('tp'), may hold values from 0.3 to 3
- down_weight: float32 [6144, 2048], P('tp', 'fs'), may hold values from -0.078125 to 0.078125
- down_scale: float32 [2048], P('fs'), may hold values from 0.3 to 3
- query_weight: float32 [2048, 2048], P('fs', 'tp'), may hold values from -0.125 to 0.125
- query_scale: float32 [2048], P('tp'), may hold values from 0.3 to 3
- key_weight: float32 [2048, 2048], P('fs', 'tp'), may hold values from -0.125 to 0.125
- key_scale: float32 [2048], P('tp'), may hold values from 0.3 to 3
- value_weight: float32 [2048, 2048], P('fs', 'tp'), may hold values from -0.125 to 0.125
- value_scale: float32 [2048], P('tp'), may hold values from 0.3 to 3
- output_weight: float32 [2048, 2048], P('tp', 'fs'), may hold values from -0.125 to 0.125
- output_scale: float32 [2048], P('fs'), may hold values from 0.3 to 3
Outputs:
- residual_out: bfloat16 [4096, 2048], P(('fs', 'tp'))
All inputs are finite; a program needn't handle non-finite values.
Results may differ from a plain program's by a relative error of at most 0.028.
Values may be sent and summed in bfloat16 or wider, within the bound.
A program may use at most 128 MiB of HBM per device.

v0:
```python
import jax
import jax.numpy as jnp
from jax import lax
from jax.sharding import PartitionSpec as P

HEADS = 8
HEAD_DIM = 256
BLOCK = 64
EPSILON = 1e-06
HEAD_FLOOR = 0.25
ROTARY_BASE = 10000.0
HIGHEST = lax.Precision.HIGHEST


def normalize(sequence_rows, gain_vector):
    values = sequence_rows.astype(jnp.float32)
    scaled = values * lax.rsqrt(jnp.mean(values * values, axis=-1, keepdims=True) + EPSILON)
    return (scaled * gain_vector).astype(jnp.bfloat16)


def collect_rows(sequence_rows, gain_vector):
    return lax.all_gather(normalize(sequence_rows, gain_vector), "tp", axis=0, tiled=True)


def return_rows(inputs, weight, factor):
    term = jnp.dot(inputs, weight, preferred_element_type=jnp.float32) * factor
    return lax.psum_scatter(
        lax.optimization_barrier(term.astype(jnp.bfloat16))
        .astype(jnp.float32)
        .astype(jnp.bfloat16),
        "tp",
        scatter_dimension=0,
        tiled=True,
    ).astype(jnp.float32)


def head_rates(first_head, head_count, length):
    head_number = (first_head + jnp.arange(head_count)).astype(jnp.float32)
    return jnp.exp(jnp.log(1.0 / 16.0) + head_number / (HEADS - 1) * jnp.log(4.0 / length))


def rotate(values, positions):
    half_width = values.shape[-1] // 2
    frequency = ROTARY_BASE ** (-jnp.arange(half_width, dtype=jnp.float32) * 2.0 / values.shape[-1])
    angles = positions[:, None] * frequency[None, :]
    cosine = jnp.cos(angles)[:, None, :]
    sine_value = jnp.sin(angles)[:, None, :]
    front_half = values[..., :half_width]
    back_half = values[..., half_width:]
    return jnp.concatenate(
        [
            front_half * cosine - back_half * sine_value,
            back_half * cosine + front_half * sine_value,
        ],
        axis=-1,
    )


def retention(query_pre, key_pre, value_pre, decay_rates):
    length, head_count, head_width = query_pre.shape
    positions = jnp.arange(length, dtype=jnp.float32)
    query_rot = rotate(query_pre, positions).astype(jnp.bfloat16)
    key_rot = rotate(key_pre, positions).astype(jnp.bfloat16)
    value_low = value_pre.astype(jnp.bfloat16)
    blocks = length // BLOCK
    inside = jnp.arange(BLOCK, dtype=jnp.float32)
    distance = inside[:, None] - inside[None, :]
    within = jnp.where(
        distance >= 0, jnp.exp(-decay_rates[:, None, None] * jnp.maximum(distance, 0.0)), 0.0
    ) * head_width ** (-0.5)
    query_blocks = query_rot.reshape(blocks, BLOCK, head_count, head_width)
    key_blocks = key_rot.reshape(blocks, BLOCK, head_count, head_width)
    value_blocks = value_low.reshape(blocks, BLOCK, head_count, head_width)
    scores = jnp.einsum(
        "nihe,njhe->nhij", query_blocks, key_blocks, preferred_element_type=jnp.float32
    )
    weights = (scores * within[None]).astype(jnp.bfloat16)
    inner_part = jnp.einsum(
        "nhij,njhe->nihe", weights, value_blocks, preferred_element_type=jnp.float32
    )
    fading = jnp.exp(-decay_rates[None, :] * (BLOCK - 1.0 - inside[:, None])) * head_width ** (-0.5)
    key_faded = key_blocks.astype(jnp.float32) * fading[None, :, :, None]
    updates = jnp.einsum(
        "njhd,njhe->nhde", key_faded, value_blocks.astype(jnp.float32), precision=HIGHEST
    )
    block_decay = jnp.exp(-decay_rates * BLOCK)

    def advance(memory_state, update):
        return (memory_state * block_decay[:, None, None] + update, memory_state)

    _, before = lax.scan(
        advance, jnp.zeros((head_count, head_width, head_width), jnp.float32), updates
    )
    rising = jnp.exp(-decay_rates[None, :] * (inside[:, None] + 1.0))
    queried = query_blocks.astype(jnp.float32) * rising[None, :, :, None]
    carried_part = jnp.einsum("nihd,nhde->nihe", queried, before, precision=HIGHEST)
    combined = (inner_part + carried_part).reshape(length, head_count, head_width)
    normed = combined * lax.rsqrt(
        jnp.maximum(jnp.mean(combined * combined, axis=-1, keepdims=True), HEAD_FLOOR)
    )
    return normed.astype(jnp.bfloat16).reshape(length, head_count * head_width)


def body(
    residual_in,
    gain_first,
    gain_mixer,
    gain_second,
    gate_weight,
    gate_scale,
    up_weight,
    up_scale,
    down_weight,
    down_scale,
    query_weight,
    query_scale,
    key_weight,
    key_scale,
    value_weight,
    value_scale,
    output_weight,
    output_scale,
):
    gate_part = gate_weight.astype(jnp.bfloat16)
    up_part = up_weight.astype(jnp.bfloat16)
    down_factor, output_factor = (
        lax.all_gather(down_scale, "fs", axis=0, tiled=True),
        lax.all_gather(output_scale, "fs", axis=0, tiled=True),
    )
    first_input = collect_rows(residual_in, gain_first)
    gate_full, up_full = (
        lax.all_gather(gate_part, "fs", axis=0, tiled=True),
        lax.all_gather(up_part, "fs", axis=0, tiled=True),
    )
    gate_pre = jnp.dot(first_input, gate_full, preferred_element_type=jnp.float32)
    up_pre = jnp.dot(first_input, up_full, preferred_element_type=jnp.float32)
    down_full = lax.all_gather(down_weight.astype(jnp.bfloat16), "fs", axis=1, tiled=True)
    hidden_first = (jax.nn.silu(gate_pre * gate_scale) * (up_pre * up_scale)).astype(jnp.bfloat16)
    mlp_first = return_rows(hidden_first, down_full, down_factor)
    middle = (residual_in.astype(jnp.float32) + 0.5 * mlp_first).astype(jnp.bfloat16)
    mixer_input = collect_rows(middle, gain_mixer)
    local_width = query_weight.shape[1]
    projections = (
        query_weight.astype(jnp.bfloat16),
        key_weight.astype(jnp.bfloat16),
        value_weight.astype(jnp.bfloat16),
    )
    pieces = (
        lax.all_gather(projections[0], "fs", axis=0, tiled=True),
        lax.all_gather(projections[1], "fs", axis=0, tiled=True),
        lax.all_gather(projections[2], "fs", axis=0, tiled=True),
    )
    query_pre, key_pre, value_pre = tuple(
        (
            jnp.dot(mixer_input, pieces[member], preferred_element_type=jnp.float32)
            for member in range(3)
        )
    )
    output_full = lax.all_gather(output_weight.astype(jnp.bfloat16), "fs", axis=1, tiled=True)
    length = mixer_input.shape[0]
    heads_local = local_width // HEAD_DIM
    decay_rates = head_rates(lax.axis_index("tp") * heads_local, heads_local, length)
    mixed = retention(
        (query_pre * query_scale).reshape(length, heads_local, HEAD_DIM),
        (key_pre * key_scale).reshape(length, heads_local, HEAD_DIM),
        (value_pre * value_scale).reshape(length, heads_local, HEAD_DIM),
        decay_rates,
    )
    mixer_out = return_rows(mixed, output_full, output_factor)
    second = (middle.astype(jnp.float32) + mixer_out).astype(jnp.bfloat16)
    last_input = collect_rows(second, gain_second)
    gate_last = jnp.dot(last_input, gate_full, preferred_element_type=jnp.float32) * gate_scale
    up_last = jnp.dot(last_input, up_full, preferred_element_type=jnp.float32) * up_scale
    hidden_second = (jax.nn.silu(gate_last) * up_last).astype(jnp.bfloat16)
    mlp_second = return_rows(hidden_second, down_full, down_factor)
    return (second.astype(jnp.float32) + 0.5 * mlp_second).astype(jnp.bfloat16)


def solution(mesh):
    in_specs = (
        P(("fs", "tp"), None),
        P(),
        P(),
        P(),
        P("fs", "tp"),
        P("tp"),
        P("fs", "tp"),
        P("tp"),
        P("tp", "fs"),
        P("fs"),
        P("fs", "tp"),
        P("tp"),
        P("fs", "tp"),
        P("tp"),
        P("fs", "tp"),
        P("tp"),
        P("tp", "fs"),
        P("fs"),
    )
    out_specs = P(("fs", "tp"), None)
    return jax.shard_map(body, mesh=mesh, in_specs=in_specs, out_specs=out_specs, check_vma=False)
```

profile of v0, /device:TPU:0, one launch (start us, length us, event | category | flops | bytes accessed | tf_op | source)
XLA Modules:
  0.0 955.4 jit_solution(6325975038016141110)
XLA Ops:
  6.5 1.3 fusion.12
  7.9 2.0 fusion.14
  10.0 2.4 convert_element_type.119
  12.5 1.0 convert_element_type.120
  13.5 0.0 all-gather.19.cloned.1.call-start
  13.6 2.4 convert_element_type.122
  16.0 43.0 %all-gather = f32[16,1,128]{2,1,0:T(1,128)S(1)} all-gather(f32[1,1,128]{2,1,0:T(1,128)S(1)} %bitcast.58), channel_id=1, replica_groups=mesh['fs'=16,'tp'=2] {'fs'}, dimensions={0}, use_global_device_ids=true | all-gather | bytes 8704 | tf_op jit(solution)/shard_map/all_gather | solution.py:127
  59.0 118.3 %all-gather.15.cloned.1.call-done = bf16[2048,3072]{1,0:T(8,128)(2,1)} async-done(((bf16[128,3072]{1,0:T(8,128)(2,1)}), bf16[2048,3072]{1,0:T(8,128)(2,1)}) %all-gather.15.cloned.1.call-update) | async-done | bytes 12582928 | tf_op jit(solution)/shard_map/all_gather | solution.py:132
  177.3 9.9 %convolution_multiply_fusion.3 = f32[256,3072]{1,0:T(8,128)} fusion(bf16[256,2048]{1,0:T(8,128)(2,1)} %all-gather.13.cloned.1.call-done, bf16[2048,3072]{1,0:T(8,128)(2,1)} %all-gather.15.cloned.1.call-done, f32[3072]{0:T(1024)S(1)} %copy-done.20), kind=kOutput, calls=%fused_computation.7 | convolution fusion | flops 3222011904 | bytes 16789504 | tf_op jit(solution)/shard_map/dot_general | solution.py:135
  187.2 142.5 %all-gather.17.cloned.1.call-done = bf16[2048,3072]{1,0:T(8,128)(2,1)} async-done(((bf16[128,3072]{1,0:T(8,128)(2,1)}), bf16[2048,3072]{1,0:T(8,128)(2,1)}) %all-gather.17.cloned.1.call-update) | async-done | bytes 12582928 | tf_op jit(solution)/shard_map/all_gather | solution.py:133
  329.7 196.2 %all-gather.19.cloned.1.call-done = bf16[3072,2048]{1,0:T(8,128)(2,1)} async-done(((bf16[3072,128]{1,0:T(8,128)(2,1)}), bf16[3072,2048]{1,0:T(8,128)(2,1)}) %all-gather.19.cloned.1.call-update) | async-done | bytes 12582928 | tf_op jit(solution)/shard_map/all_gather | solution.py:137
  525.9 17.1 %fusion.6 = bf16[256,2048]{1,0:T(8,128)(2,1)} fusion(bf16[3072,2048]{1,0:T(8,128)(2,1)} %all-gather.19.cloned.1.call-done, f32[2048]{0:T(1024)S(1)} %bitcast.56, bf16[256,2048]{1,0:T(8,128)(2,1)S(1)} %copy-done.18, bf16[2048,3072]{1,0:T(8,128)(2,1)} %all-gather.17.cloned.1.call-done, f32[256,3072]{1,0:T(8,128)} %convolution_multiply_fusion.3, ...), kind=kOutput, calls=%fused_computation.15 | convolution fusion | flops 6449004544 | bytes 30429184 | tf_op jit(solution)/shard_map/dot_general | solution.py:26
  543.2 0.7 convert_element_type.131
  543.9 0.0 all-gather.21.cloned.1.call-start
  544.0 5.9 reduce-scatter.4.cloned.1.call-done
  549.8 1.3 fusion.16
  551.2 1.0 fusion.18
  552.3 0.8 convert_element_type.132
  553.1 0.7 convert_element_type.128
  553.9 0.7 convert_element_type.138
  554.8 41.1 %all-gather.1 = f32[16,1,128]{2,1,0:T(1,128)S(1)} all-gather(f32[1,1,128]{2,1,0:T(1,128)S(1)} %bitcast.59), channel_id=1, replica_groups=mesh['fs'=16,'tp'=2] {'fs'}, dimensions={0}, use_global_device_ids=true | all-gather | bytes 8704 | tf_op jit(solution)/shard_map/all_gather | solution.py:128
  596.0 0.1 multiply_exponential_fusion.1
  596.1 0.7 select_multiply_fusion
  596.8 1.1 fusion.42
  598.0 31.3 %all-gather.25.cloned.1.call-done = bf16[2048,1024]{1,0:T(8,128)(2,1)} async-done(((bf16[128,1024]{1,0:T(8,128)(2,1)}), bf16[2048,1024]{1,0:T(8,128)(2,1)}) %all-gather.25.cloned.1.call-update) | async-done | bytes 4194320 | tf_op jit(solution)/shard_map/all_gather | solution.py:149
  629.2 9.2 all-gather.21.cloned.1.call-done
  638.4 4.7 convolution_multiply_fusion.8
  643.2 1.7 reshape.230
  644.9 73.1 %all-gather.27.cloned.1.call-done = bf16[2048,1024]{1,0:T(8,128)(2,1)} async-done(((bf16[128,1024]{1,0:T(8,128)(2,1)}), bf16[2048,1024]{1,0:T(8,128)(2,1)}) %all-gather.27.cloned.1.call-update) | async-done | bytes 4194320 | tf_op jit(solution)/shard_map/all_gather | solution.py:150
  718.0 4.7 convolution_multiply_fusion.7
  722.7 2.7 reshape.231
  725.4 69.6 %all-gather.23.cloned.1.call-done = bf16[2048,1024]{1,0:T(8,128)(2,1)} async-done(((bf16[128,1024]{1,0:T(8,128)(2,1)}), bf16[2048,1024]{1,0:T(8,128)(2,1)}) %all-gather.23.cloned.1.call-update) | async-done | bytes 4194320 | tf_op jit(solution)/shard_map/all_gather | solution.py:151
  795.0 4.6 fusion.10
  799.5 1.4 convert_element_type.130
  801.0 1.5 fusion.48
  802.5 0.3 subtract_convert_fusion.1
  802.8 3.9 fusion.27
  806.7 10.4 %while.13 = (s32[]{:T(128)}, f32[4,256,256]{2,1,0:T(8,128)S(1)}, f32[4,4,256,256]{3,2,1,0:T(8,128)}, f32[4,4,256,256]{3,2,1,0:T(8,128)}, s32[]{:T(128)}, /*index=5*/s32[]{:T(128)}, s32[]{:T(128)}) while((s32[]{:T(128)}, f32[4,256,256]{2,1,0:T(8,128)S(1)}, f32[4,4,256,256]{3,2,1,0:T(8,128)}, f32[4,4,256,256]{3,2,1,0:T(8,128)}, ...), condition=%wide.region_4.5_spmd.clone, body=%wide.region_3.4_spmd.clone.sunk | while | flops 1048603 | bytes 5243520 | solution.py:91
  806.7 1.1 bitcast_dynamic-update-slice_fusion.2
  807.8 1.5 bitcast_add_fusion.2
  809.3 1.1 bitcast_dynamic-update-slice_fusion.2
  810.4 1.5 bitcast_add_fusion.2
  811.9 1.1 bitcast_dynamic-update-slice_fusion.2
  813.0 1.5 bitcast_add_fusion.2
  814.5 1.1 bitcast_dynamic-update-slice_fusion.2
  815.7 1.5 bitcast_add_fusion.2
  817.2 5.1 fusion.24
  822.3 1.6 multiply_reduce_fusion
  824.0 0.1 copy.52
  824.1 0.3 mul.482
  824.4 0.2 copy.59
  824.6 0.7 copy.47
  825.3 0.2 copy.58
  825.5 59.4 %all-gather.29.cloned.1.call-done = bf16[1024,2048]{1,0:T(8,128)(2,1)} async-done(((bf16[1024,128]{1,0:T(8,128)(2,1)}), bf16[1024,2048]{1,0:T(8,128)(2,1)}) %all-gather.29.cloned.1.call-update) | async-done | bytes 4194320 | tf_op jit(solution)/shard_map/all_gather | solution.py:159
  884.9 4.5 fusion.8
  889.5 6.7 reduce-scatter.6.cloned.1.call-done
  896.2 1.3 fusion.20
  897.5 2.0 fusion.22
  899.6 0.3 reduce-scatter.8.cloned.1.call-start
  899.9 10.1 %all-gather.31.cloned.1.call-done = bf16[256,2048]{1,0:T(8,128)(2,1)} async-done(((bf16[128,2048]{1,0:T(8,128)(2,1)}), bf16[256,2048]{1,0:T(8,128)(2,1)}) %all-gather.31.cloned.1.call-update) | async-done | bytes 1048592 | tf_op jit(solution)/shard_map/all_gather | solution.py:22
  909.9 10.0 %convolution_multiply_fusion.1 = f32[256,3072]{1,0:T(8,128)} fusion(bf16[256,2048]{1,0:T(8,128)(2,1)} %all-gather.31.cloned.1.call-done, bf16[2048,3072]{1,0:T(8,128)(2,1)} %all-gather.15.cloned.1.call-done, f32[3072]{0:T(1024)S(1)} %copy-done.21), kind=kOutput, calls=%fused_computation.5 | convolution fusion | flops 3222011904 | bytes 16789504 | tf_op jit(solution)/shard_map/dot_general | solution.py:172
  920.0 17.0 %fusion.7 = bf16[256,2048]{1,0:T(8,128)(2,1)} fusion(bf16[3072,2048]{1,0:T(8,128)(2,1)} %all-gather.19.cloned.1.call-done, f32[2048]{0:T(1024)S(1)} %bitcast.57, bf16[256,2048]{1,0:T(8,128)(2,1)S(1)} %copy-done.19, bf16[2048,3072]{1,0:T(8,128)(2,1)} %all-gather.17.cloned.1.call-done, f32[256,3072]{1,0:T(8,128)} %convolution_multiply_fusion.1, ...), kind=kOutput, calls=%fused_computation.16 | convolution fusion | flops 6449004544 | bytes 30429184 | tf_op jit(solution)/shard_map/dot_general | solution.py:26
  937.0 9.7 %reduce-scatter.8.cloned.1.call-done = bf16[128,2048]{1,0:T(8,128)(2,1)} async-done(((bf16[256,2048]{1,0:T(8,128)(2,1)}), bf16[128,2048]{1,0:T(8,128)(2,1)}) %reduce-scatter.8.cloned.1.call-update) | async-done | bytes 524304 | tf_op jit(solution)/shard_map/reduce_scatter | solution.py:27
  946.8 2.1 fusion.23
  (93 shorter events, 0.9 us)
Async XLA Ops:
  6.5 5.9 copy-start.2
  6.5 52.5 %all-gather.13.cloned.1.call-start = ((), (), s32[]{:S(2)}) async-start(), calls=%async_computation.3 | async-start | bytes 1572864 | tf_op jit(solution)/shard_map/all_gather | solution.py:22
  9.9 6.1 copy-start.16
  10.0 167.3 %copy-start.20 = (f32[3072]{0:T(1024)S(1)}, f32[3072]{0:T(1024)}, u32[]{:S(2)}) copy-start(f32[3072]{0:T(1024)} %param.25) | copy-start | bytes 36868
  10.0 167.3 %all-gather.15.cloned.1.call-start = ((), (), s32[]{:S(2)}) async-start(), calls=%async_computation.4 | async-start | bytes 13369344 | tf_op jit(solution)/shard_map/all_gather | solution.py:132
  12.4 317.3 %all-gather.17.cloned.1.call-start = ((), (), s32[]{:S(2)}) async-start(), calls=%async_computation.5 | async-start | bytes 13369344 | tf_op jit(solution)/shard_map/all_gather | solution.py:133
  13.5 512.4 %all-gather.19.cloned.1.call-start = ((), (), s32[]{:S(2)}) async-start(), calls=%async_computation.6 | async-start | bytes 13369344 | tf_op jit(solution)/shard_map/all_gather | solution.py:137
  16.0 533.8 %reduce-scatter.4.cloned.1.call-start = ((), (), s32[]{:S(2)}) async-start(), calls=%async_computation.7 | async-start | bytes 1572864 | tf_op jit(solution)/shard_map/reduce_scatter | solution.py:27
  59.0 466.9 %copy-start.14 = (f32[16,1,128]{2,1,0:T(1,128)}, f32[16,1,128]{2,1,0:T(1,128)S(1)}, u32[]{:S(2)}) copy-start(f32[16,1,128]{2,1,0:T(1,128)S(1)} %all-gather) | copy-start | bytes 24580
  59.0 466.9 %copy-start.22 = (f32[3072]{0:T(1024)S(1)}, f32[3072]{0:T(1024)}, u32[]{:S(2)}) copy-start(f32[3072]{0:T(1024)} %param.27) | copy-start | bytes 36868
  59.0 466.9 %copy-start.18 = (bf16[256,2048]{1,0:T(8,128)(2,1)S(1)}, bf16[256,2048]{1,0:T(8,128)(2,1)}, u32[]{:S(2)}) copy-start(bf16[256,2048]{1,0:T(8,128)(2,1)} %all-gather.13.cloned.1.call-done) | copy-start | bytes 3145732
  525.9 17.2 %copy-start.6 = (f32[128,1024]{1,0:T(8,128)S(1)}, f32[128,1024]{1,0:T(8,128)}, u32[]{:S(2)}) copy-start(f32[128,1024]{1,0:T(8,128)} %param.30) | copy-start | bytes 1572868
  525.9 23.9 %copy-start = (bf16[128,2048]{1,0:T(8,128)(2,1)S(1)}, bf16[128,2048]{1,0:T(8,128)(2,1)}, u32[]{:S(2)}) copy-start(bf16[128,2048]{1,0:T(8,128)(2,1)} %param.20) | copy-start | bytes 1572868
  525.9 25.2 %copy-start.12 = (f32[2048]{0:T(1024)S(1)}, f32[2048]{0:T(1024)}, u32[]{:S(2)}) copy-start(f32[2048]{0:T(1024)} %param.22) | copy-start | bytes 24580
  543.0 9.2 copy-start.7
  543.0 10.0 %copy-start.8 = (f32[128,1024]{1,0:T(8,128)S(1)}, f32[128,1024]{1,0:T(8,128)}, u32[]{:S(2)}) copy-start(f32[128,1024]{1,0:T(8,128)} %param.34) | copy-start | bytes 1572868
  543.0 10.9 %copy-start.9 = (f32[1024,128]{1,0:T(8,128)S(1)}, f32[1024,128]{1,0:T(8,128)}, u32[]{:S(2)}) copy-start(f32[1024,128]{1,0:T(8,128)} %param.36) | copy-start | bytes 1572868
  543.0 11.7 %copy-start.17 = (f32[128]{0:T(128)S(1)}, f32[128]{0:T(128)}, u32[]{:S(2)}) copy-start(f32[128]{0:T(128)} %param.37) | copy-start | bytes 1540
  543.1 95.3 %copy-start.24 = (f32[1024]{0:T(1024)S(1)}, f32[1024]{0:T(1024)}, u32[]{:S(2)}) copy-start(f32[1024]{0:T(1024)} %param.31) | copy-start | bytes 12292
  543.1 86.1 %all-gather.25.cloned.1.call-start = ((), (), s32[]{:S(2)}) async-start(), calls=%async_computation.10 | async-start | bytes 4456448 | tf_op jit(solution)/shard_map/all_gather | solution.py:149
  543.9 94.5 %all-gather.21.cloned.1.call-start = ((), (), s32[]{:S(2)}) async-start(), calls=%async_computation.8 | async-start | bytes 1572864 | tf_op jit(solution)/shard_map/all_gather | solution.py:22
  552.2 165.8 %all-gather.27.cloned.1.call-start = ((), (), s32[]{:S(2)}) async-start(), calls=%async_computation.11 | async-start | bytes 4456448 | tf_op jit(solution)/shard_map/all_gather | solution.py:150
  553.0 242.0 %all-gather.23.cloned.1.call-start = ((), (), s32[]{:S(2)}) async-start(), calls=%async_computation.9 | async-start | bytes 4456448 | tf_op jit(solution)/shard_map/all_gather | solution.py:151
  553.9 331.1 %all-gather.29.cloned.1.call-start = ((), (), s32[]{:S(2)}) async-start(), calls=%async_computation.12 | async-start | bytes 4456448 | tf_op jit(solution)/shard_map/all_gather | solution.py:159
  554.7 341.5 %reduce-scatter.6.cloned.1.call-start = ((), (), s32[]{:S(2)}) async-start(), calls=%async_computation.13 | async-start | bytes 1572864 | tf_op jit(solution)/shard_map/reduce_scatter | solution.py:27
  598.0 120.0 %copy-start.25 = (f32[1024]{0:T(1024)S(1)}, f32[1024]{0:T(1024)}, u32[]{:S(2)}) copy-start(f32[1024]{0:T(1024)} %param.33) | copy-start | bytes 12292
  644.9 150.1 %copy-start.26 = (f32[1024]{0:T(1024)S(1)}, f32[1024]{0:T(1024)}, u32[]{:S(2)}) copy-start(f32[1024]{0:T(1024)} %param.35) | copy-start | bytes 12292
  801.0 1.5 copy-start.10
  802.8 4.0 copy-start.3
  802.8 14.4 %copy-start.4 = (bf16[256,4,128]{2,0,1:T(8,128)(2,1)}, bf16[256,4,128]{2,0,1:T(8,128)(2,1)S(1)}, u32[]{:S(2)}) copy-start(bf16[256,4,128]{2,0,1:T(8,128)(2,1)S(1)} %get-tuple-element.66) | copy-start | bytes 786436
  802.8 14.4 %copy-start.5 = (bf16[256,4,128]{2,0,1:T(8,128)(2,1)}, bf16[256,4,128]{2,0,1:T(8,128)(2,1)S(1)}, u32[]{:S(2)}) copy-start(bf16[256,4,128]{2,0,1:T(8,128)(2,1)S(1)} %get-tuple-element.67) | copy-start | bytes 786436
  817.1 5.2 copy-start.11
  884.9 12.5 %copy-start.13 = (f32[2048]{0:T(1024)S(1)}, f32[2048]{0:T(1024)}, u32[]{:S(2)}) copy-start(f32[2048]{0:T(1024)} %param.23) | copy-start | bytes 24580
  884.9 25.0 %copy-start.21 = (f32[3072]{0:T(1024)S(1)}, f32[3072]{0:T(1024)}, u32[]{:S(2)}) copy-start(f32[3072]{0:T(1024)} %param.25) | copy-start | bytes 36868
  889.4 20.5 %all-gather.31.cloned.1.call-start = ((), (), s32[]{:S(2)}) async-start(), calls=%async_computation.14 | async-start | bytes 1572864 | tf_op jit(solution)/shard_map/all_gather | solution.py:22
  899.5 20.4 %copy-start.15 = (f32[16,1,128]{2,1,0:T(1,128)S(1)}, f32[16,1,128]{2,1,0:T(1,128)}, u32[]{:S(2)}) copy-start(f32[16,1,128]{2,1,0:T(1,128)} %copy-done.14) | copy-start | bytes 24580
  899.5 20.4 %copy-start.23 = (f32[3072]{0:T(1024)S(1)}, f32[3072]{0:T(1024)}, u32[]{:S(2)}) copy-start(f32[3072]{0:T(1024)} %param.27) | copy-start | bytes 36868
  899.6 47.2 %reduce-scatter.8.cloned.1.call-start = ((), (), s32[]{:S(2)}) async-start(), calls=%async_computation.15 | async-start | bytes 1572864 | tf_op jit(solution)/shard_map/reduce_scatter | solution.py:27
  909.9 10.0 %copy-start.19 = (bf16[256,2048]{1,0:T(8,128)(2,1)S(1)}, bf16[256,2048]{1,0:T(8,128)(2,1)}, u32[]{:S(2)}) copy-start(bf16[256,2048]{1,0:T(8,128)(2,1)} %all-gather.31.cloned.1.call-done) | copy-start | bytes 3145732
  920.0 26.8 %copy-start.1 = (bf16[128,2048]{1,0:T(8,128)(2,1)S(1)}, bf16[128,2048]{1,0:T(8,128)(2,1)}, u32[]{:S(2)}) copy-start(bf16[128,2048]{1,0:T(8,128)(2,1)} %reduce-scatter.6.cloned.1.call-done) | copy-start | bytes 1572868
Sparse Core Ops, SparseCore 0:
  10.1 11.7 all-gather.12
  24.6 152.6 all-gather.14
  180.1 149.5 all-gather.16
  332.2 193.6 all-gather.18
  543.2 6.5 reduce-scatter.3
  552.4 76.7 all-gather.24
  630.8 7.6 all-gather.20
  641.2 76.7 all-gather.26
  720.8 74.1 all-gather.22
  797.5 87.3 all-gather.28
  889.6 6.5 reduce-scatter.5
  899.7 10.2 all-gather.30
  937.1 9.5 reduce-scatter.7
where the time goes:
time: 956 us; the launch traced here: 955 us
  waiting for transfers between devices  732 us (77%)
  blocking collectives  84.1 us (9%)
  matrix products  83.2 us (9%)
  other arithmetic  32.5 us (3%)
  between operations  13.6 us (1%)
    all_gather x1, waiting for transfers between devices, body(): lax.all_gather(down_weight.astype(jnp.bfloat16), 'fs', axis=1, tiled=True)  196 us
    all_gather x1, waiting for transfers between devices, body(): lax.all_gather(up_part, 'fs', axis=0, tiled=True)  142 us
    all_gather x1, waiting for transfers between devices, body(): lax.all_gather(gate_part, 'fs', axis=0, tiled=True)  118 us
    all_gather x1, waiting for transfers between devices, body(): lax.all_gather(projections[1], 'fs', axis=0, tiled=True)  73.1 us
    all_gather x1, waiting for transfers between devices, body(): lax.all_gather(projections[2], 'fs', axis=0, tiled=True)  69.6 us
    all_gather x1, waiting for transfers between devices, body(): lax.all_gather(output_weight.astype(jnp.bfloat16), 'fs', axis=1, tiled=True)  59.4 us
    all_gather x1, blocking collectives, body(): lax.all_gather(down_scale, 'fs', axis=0, tiled=True)  43 us
    all_gather x1, blocking collectives, body(): lax.all_gather(output_scale, 'fs', axis=0, tiled=True)  41.1 us
  transfers between devices with their start and end apart: 13, of which 12 were waited for; matrix products, arithmetic and copies ran while one was open for 7% of the time, Pallas kernels for 0%

commit v1 on v0

--- a/solution.py
+++ b/solution.py
@@ -156,7 +156,7 @@
             for member in range(3)
         )
     )
-    output_full = lax.all_gather(output_weight.astype(jnp.bfloat16), "fs", axis=1, tiled=True)
+    output_full = jnp.concatenate(lax.all_gather(output_weight.astype(jnp.bfloat16), "fs"), axis=1)
     length = mixer_input.shape[0]
     heads_local = local_width // HEAD_DIM
     decay_rates = head_rates(lax.axis_index("tp") * heads_local, heads_local, length)

time: 956 us -> 975 us (1.020)
  waiting for transfers between devices: 732 us -> 742 us
    all_gather x1, waiting for transfers between devices: 31.3 us -> 70.6 us  [body(): lax.all_gather(projections[0], 'fs', axis=0, tiled=True)]
    all_gather x1, waiting for transfers between devices: 59.4 us -> 30.9 us  [body(): lax.all_gather(output_weight.astype(jnp.bfloat16), 'fs')]
  transfers between devices with their start and end apart: 13 -> 13, of which waited for: 12 -> 12; matrix products, arithmetic and copies ran while one was open for 7% -> 4% of each run, Pallas kernels for 0% -> 0%
where the time goes in v1:
time: 975 us; the launch traced here: 974 us
  waiting for transfers between devices  742 us (76%)
  blocking collectives  85.4 us (9%)
  matrix products  83.9 us (9%)
  other arithmetic  34.3 us (4%)
  local copies, waits for them, and re-layouts  14.3 us (1%)
  between operations  13.6 us (1%)
    all_gather x1, waiting for transfers between devices, body(): lax.all_gather(down_weight.astype(jnp.bfloat16), 'fs', axis=1, tiled=True)  196 us
    all_gather x1, waiting for transfers between devices, body(): lax.all_gather(up_part, 'fs', axis=0, tiled=True)  142 us
    all_gather x1, waiting for transfers between devices, body(): lax.all_gather(gate_part, 'fs', axis=0, tiled=True)  118 us
    all_gather x1, waiting for transfers between devices, body(): lax.all_gather(projections[1], 'fs', axis=0, tiled=True)  73.1 us
    all_gather x1, waiting for transfers between devices, body(): lax.all_gather(projections[0], 'fs', axis=0, tiled=True)  70.6 us
    all_gather x1, waiting for transfers between devices, body(): lax.all_gather(projections[2], 'fs', axis=0, tiled=True)  69.4 us
    all_gather x1, blocking collectives, body(): lax.all_gather(down_scale, 'fs', axis=0, tiled=True)  43 us
    all_gather x1, blocking collectives, body(): lax.all_gather(output_scale, 'fs', axis=0, tiled=True)  42.4 us
  transfers between devices with their start and end apart: 13, of which 12 were waited for; matrix products, arithmetic and copies ran while one was open for 4% of the time, Pallas kernels for 0%

profile of v1, /device:TPU:0, one launch (start us, length us, event | category | flops | bytes accessed | tf_op | source)
XLA Modules:
  0.0 974.5 jit_solution(3764712087428823473)
XLA Ops:
  6.5 1.3 fusion.12
  7.9 2.0 fusion.14
  10.0 2.4 convert_element_type.122
  12.5 1.0 convert_element_type.123
  13.6 0.0 all-gather.20.cloned.1.call-start
  13.6 2.4 convert_element_type.125
  16.1 43.0 %all-gather.1 = f32[16,1,128]{2,1,0:T(1,128)S(1)} all-gather(f32[1,1,128]{2,1,0:T(1,128)S(1)} %bitcast.59), channel_id=1, replica_groups=mesh['fs'=16,'tp'=2] {'fs'}, dimensions={0}, use_global_device_ids=true | all-gather | bytes 8704 | tf_op jit(solution)/shard_map/all_gather | solution.py:127
  59.1 118.2 %all-gather.16.cloned.1.call-done = bf16[2048,3072]{1,0:T(8,128)(2,1)} async-done(((bf16[128,3072]{1,0:T(8,128)(2,1)}), bf16[2048,3072]{1,0:T(8,128)(2,1)}) %all-gather.16.cloned.1.call-update) | async-done | bytes 12582928 | tf_op jit(solution)/shard_map/all_gather | solution.py:132
  177.3 9.9 %convolution_multiply_fusion.3 = f32[256,3072]{1,0:T(8,128)} fusion(bf16[256,2048]{1,0:T(8,128)(2,1)} %all-gather.14.cloned.1.call-done, bf16[2048,3072]{1,0:T(8,128)(2,1)} %all-gather.16.cloned.1.call-done, f32[3072]{0:T(1024)S(1)} %copy-done.17), kind=kOutput, calls=%fused_computation.7 | convolution fusion | flops 3222011904 | bytes 16789504 | tf_op jit(solution)/shard_map/dot_general | solution.py:135
  187.2 142.5 %all-gather.18.cloned.1.call-done = bf16[2048,3072]{1,0:T(8,128)(2,1)} async-done(((bf16[128,3072]{1,0:T(8,128)(2,1)}), bf16[2048,3072]{1,0:T(8,128)(2,1)}) %all-gather.18.cloned.1.call-update) | async-done | bytes 12582928 | tf_op jit(solution)/shard_map/all_gather | solution.py:133
  329.7 196.2 %all-gather.20.cloned.1.call-done = bf16[3072,2048]{1,0:T(8,128)(2,1)} async-done(((bf16[3072,128]{1,0:T(8,128)(2,1)}), bf16[3072,2048]{1,0:T(8,128)(2,1)}) %all-gather.20.cloned.1.call-update) | async-done | bytes 12582928 | tf_op jit(solution)/shard_map/all_gather | solution.py:137
  525.9 17.1 %fusion.6 = bf16[256,2048]{1,0:T(8,128)(2,1)} fusion(bf16[3072,2048]{1,0:T(8,128)(2,1)} %all-gather.20.cloned.1.call-done, f32[2048]{0:T(1024)S(1)} %bitcast.56, bf16[256,2048]{1,0:T(8,128)(2,1)S(1)} %copy-done.15, bf16[2048,3072]{1,0:T(8,128)(2,1)} %all-gather.18.cloned.1.call-done, f32[256,3072]{1,0:T(8,128)} %convolution_multiply_fusion.3, ...), kind=kOutput, calls=%fused_computation.15 | convolution fusion | flops 6449004544 | bytes 30429184 | tf_op jit(solution)/shard_map/dot_general | solution.py:26
  543.1 0.8 convert_element_type.142
  543.9 0.7 convert_element_type.134
  544.7 0.0 all-gather.22.cloned.1.call-start
  544.8 5.0 reduce-scatter.4.cloned.1.call-done
  549.8 1.3 fusion.16
  551.1 1.0 fusion.18
  552.2 0.7 convert_element_type.135
  553.0 0.7 convert_element_type.131
  553.9 42.4 %all-gather.2 = f32[16,1,128]{2,1,0:T(1,128)} all-gather(f32[1,1,128]{2,1,0:T(1,128)S(1)} %bitcast.60), channel_id=1, replica_groups=mesh['fs'=16,'tp'=2] {'fs'}, dimensions={0}, use_global_device_ids=true | all-gather | bytes 8704 | tf_op jit(solution)/shard_map/all_gather | solution.py:128
  596.4 0.1 multiply_exponential_fusion.1
  596.5 0.8 select_multiply_fusion
  597.2 1.2 fusion.42
  598.4 30.9 %all-gather.32.cloned.1.call-done = bf16[16384,128]{1,0:T(8,128)(2,1)} async-done(((bf16[1024,128]{1,0:T(8,128)(2,1)}), bf16[16384,128]{1,0:T(8,128)(2,1)}) %all-gather.32.cloned.1.call-update) | async-done | bytes 4194320 | tf_op jit(solution)/shard_map/all_gather | solution.py:159
  629.3 6.4 copy.61
  635.7 70.6 %all-gather.26.cloned.1.call-done = bf16[2048,1024]{1,0:T(8,128)(2,1)} async-done(((bf16[128,1024]{1,0:T(8,128)(2,1)}), bf16[2048,1024]{1,0:T(8,128)(2,1)}) %all-gather.26.cloned.1.call-update) | async-done | bytes 4194320 | tf_op jit(solution)/shard_map/all_gather | solution.py:149
  706.3 9.2 all-gather.22.cloned.1.call-done
  715.5 4.8 convolution_multiply_fusion.8
  720.2 1.7 reshape.232
  721.9 73.1 %all-gather.28.cloned.1.call-done = bf16[2048,1024]{1,0:T(8,128)(2,1)} async-done(((bf16[128,1024]{1,0:T(8,128)(2,1)}), bf16[2048,1024]{1,0:T(8,128)(2,1)}) %all-gather.28.cloned.1.call-update) | async-done | bytes 4194320 | tf_op jit(solution)/shard_map/all_gather | solution.py:150
  795.0 4.7 convolution_multiply_fusion.7
  799.8 2.7 reshape.233
  802.4 69.4 %all-gather.24.cloned.1.call-done = bf16[2048,1024]{1,0:T(8,128)(2,1)} async-done(((bf16[128,1024]{1,0:T(8,128)(2,1)}), bf16[2048,1024]{1,0:T(8,128)(2,1)}) %all-gather.24.cloned.1.call-update) | async-done | bytes 4194320 | tf_op jit(solution)/shard_map/all_gather | solution.py:151
  871.9 4.6 fusion.10
  876.4 1.4 convert_element_type.133
  877.9 1.5 fusion.48
  879.4 1.1 subtract_convert_fusion.1
  880.4 4.0 fusion.27
  884.4 10.4 %while.13 = (s32[]{:T(128)}, f32[4,256,256]{2,1,0:T(8,128)S(1)}, f32[4,4,256,256]{3,2,1,0:T(8,128)}, f32[4,4,256,256]{3,2,1,0:T(8,128)}, s32[]{:T(128)}, /*index=5*/s32[]{:T(128)}, s32[]{:T(128)}) while((s32[]{:T(128)}, f32[4,256,256]{2,1,0:T(8,128)S(1)}, f32[4,4,256,256]{3,2,1,0:T(8,128)}, f32[4,4,256,256]{3,2,1,0:T(8,128)}, ...), condition=%wide.region_4.5_spmd.clone, body=%wide.region_3.4_spmd.clone.sunk | while | flops 1048603 | bytes 5243520 | solution.py:91
  884.4 1.1 bitcast_dynamic-update-slice_fusion.2
  885.5 1.5 bitcast_add_fusion.2
  887.0 1.1 bitcast_dynamic-update-slice_fusion.2
  888.1 1.5 bitcast_add_fusion.2
  889.6 1.1 bitcast_dynamic-update-slice_fusion.2
  890.7 1.5 bitcast_add_fusion.2
  892.2 1.1 bitcast_dynamic-update-slice_fusion.2
  893.3 1.5 bitcast_add_fusion.2
  894.8 5.2 fusion.24
  900.0 2.2 multiply_reduce_fusion
  902.2 0.7 maximum_rsqrt_fusion
  902.9 0.2 multiply_convert_fusion
  903.1 0.4 copy.60
  903.5 0.1 copy.68
  903.7 4.5 fusion.8
  908.2 7.1 reduce-scatter.6.cloned.1.call-done
  915.3 1.3 fusion.20
  916.6 2.0 fusion.22
  918.7 0.3 reduce-scatter.8.cloned.1.call-start
  919.0 10.1 %all-gather.30.cloned.1.call-done = bf16[256,2048]{1,0:T(8,128)(2,1)} async-done(((bf16[128,2048]{1,0:T(8,128)(2,1)}), bf16[256,2048]{1,0:T(8,128)(2,1)}) %all-gather.30.cloned.1.call-update) | async-done | bytes 1048592 | tf_op jit(solution)/shard_map/all_gather | solution.py:22
  929.1 10.0 %convolution_multiply_fusion.1 = f32[256,3072]{1,0:T(8,128)} fusion(bf16[256,2048]{1,0:T(8,128)(2,1)} %all-gather.30.cloned.1.call-done, bf16[2048,3072]{1,0:T(8,128)(2,1)} %all-gather.16.cloned.1.call-done, f32[3072]{0:T(1024)S(1)} %copy-done.18), kind=kOutput, calls=%fused_computation.5 | convolution fusion | flops 3222011904 | bytes 16789504 | tf_op jit(solution)/shard_map/dot_general | solution.py:172
  939.1 17.0 %fusion.7 = bf16[256,2048]{1,0:T(8,128)(2,1)} fusion(bf16[3072,2048]{1,0:T(8,128)(2,1)} %all-gather.20.cloned.1.call-done, f32[2048]{0:T(1024)S(1)} %bitcast.57, bf16[256,2048]{1,0:T(8,128)(2,1)S(1)} %copy-done.16, bf16[2048,3072]{1,0:T(8,128)(2,1)} %all-gather.18.cloned.1.call-done, f32[256,3072]{1,0:T(8,128)} %convolution_multiply_fusion.1, ...), kind=kOutput, calls=%fused_computation.16 | convolution fusion | flops 6449004544 | bytes 30429184 | tf_op jit(solution)/shard_map/dot_general | solution.py:26
  956.2 9.7 reduce-scatter.8.cloned.1.call-done
  965.9 2.1 fusion.23
  (86 shorter events, 0.8 us)
Async XLA Ops:
  6.5 6.0 copy-start.2
  6.5 52.6 %all-gather.14.cloned.1.call-start = ((), (), s32[]{:S(2)}) async-start(), calls=%async_computation.3 | async-start | bytes 1572864 | tf_op jit(solution)/shard_map/all_gather | solution.py:22
  9.9 6.2 copy-start.13
  10.0 167.3 %copy-start.17 = (f32[3072]{0:T(1024)S(1)}, f32[3072]{0:T(1024)}, u32[]{:S(2)}) copy-start(f32[3072]{0:T(1024)} %param.25) | copy-start | bytes 36868
  10.0 167.3 %all-gather.16.cloned.1.call-start = ((), (), s32[]{:S(2)}) async-start(), calls=%async_computation.4 | async-start | bytes 13369344 | tf_op jit(solution)/shard_map/all_gather | solution.py:132
  12.5 317.2 %all-gather.18.cloned.1.call-start = ((), (), s32[]{:S(2)}) async-start(), calls=%async_computation.5 | async-start | bytes 13369344 | tf_op jit(solution)/shard_map/all_gather | solution.py:133
  13.6 512.3 %all-gather.20.cloned.1.call-start = ((), (), s32[]{:S(2)}) async-start(), calls=%async_computation.6 | async-start | bytes 13369344 | tf_op jit(solution)/shard_map/all_gather | solution.py:137
  16.1 533.7 %reduce-scatter.4.cloned.1.call-start = ((), (), s32[]{:S(2)}) async-start(), calls=%async_computation.7 | async-start | bytes 1572864 | tf_op jit(solution)/shard_map/reduce_scatter | solution.py:27
  59.1 466.8 %copy-start.19 = (f32[3072]{0:T(1024)S(1)}, f32[3072]{0:T(1024)}, u32[]{:S(2)}) copy-start(f32[3072]{0:T(1024)} %param.27) | copy-start | bytes 36868
  59.1 466.8 %copy-start.15 = (bf16[256,2048]{1,0:T(8,128)(2,1)S(1)}, bf16[256,2048]{1,0:T(8,128)(2,1)}, u32[]{:S(2)}) copy-start(bf16[256,2048]{1,0:T(8,128)(2,1)} %all-gather.14.cloned.1.call-done) | copy-start | bytes 3145732
  525.9 17.2 %copy-start.4 = (f32[1024,128]{1,0:T(8,128)S(1)}, f32[1024,128]{1,0:T(8,128)}, u32[]{:S(2)}) copy-start(f32[1024,128]{1,0:T(8,128)} %param.36) | copy-start | bytes 1572868
  525.9 18.0 %copy-start.5 = (f32[128,1024]{1,0:T(8,128)S(1)}, f32[128,1024]{1,0:T(8,128)}, u32[]{:S(2)}) copy-start(f32[128,1024]{1,0:T(8,128)} %param.30) | copy-start | bytes 1572868
  525.9 23.9 %copy-start = (bf16[128,2048]{1,0:T(8,128)(2,1)S(1)}, bf16[128,2048]{1,0:T(8,128)(2,1)}, u32[]{:S(2)}) copy-start(bf16[128,2048]{1,0:T(8,128)(2,1)} %param.20) | copy-start | bytes 1572868
  543.0 8.1 copy-start.10
  543.0 9.2 copy-start.6
  543.0 10.0 %copy-start.7 = (f32[128,1024]{1,0:T(8,128)S(1)}, f32[128,1024]{1,0:T(8,128)}, u32[]{:S(2)}) copy-start(f32[128,1024]{1,0:T(8,128)} %param.34) | copy-start | bytes 1572868
  543.0 10.9 %copy-start.14 = (f32[128]{0:T(128)S(1)}, f32[128]{0:T(128)}, u32[]{:S(2)}) copy-start(f32[128]{0:T(128)} %param.37) | copy-start | bytes 1540
  543.0 86.2 %all-gather.32.cloned.1.call-start = ((), (), s32[]{:S(2)}) async-start(), calls=%async_computation.15 | async-start | bytes 4456448 | tf_op jit(solution)/shard_map/all_gather | solution.py:159
  543.9 162.4 %all-gather.26.cloned.1.call-start = ((), (), s32[]{:S(2)}) async-start(), calls=%async_computation.10 | async-start | bytes 4456448 | tf_op jit(solution)/shard_map/all_gather | solution.py:149
  544.7 170.7 %all-gather.22.cloned.1.call-start = ((), (), s32[]{:S(2)}) async-start(), calls=%async_computation.8 | async-start | bytes 1572864 | tf_op jit(solution)/shard_map/all_gather | solution.py:22
  552.2 242.9 %all-gather.28.cloned.1.call-start = ((), (), s32[]{:S(2)}) async-start(), calls=%async_computation.11 | async-start | bytes 4456448 | tf_op jit(solution)/shard_map/all_gather | solution.py:150
  553.0 318.9 %all-gather.24.cloned.1.call-start = ((), (), s32[]{:S(2)}) async-start(), calls=%async_computation.9 | async-start | bytes 4456448 | tf_op jit(solution)/shard_map/all_gather | solution.py:151
  553.8 361.5 %reduce-scatter.6.cloned.1.call-start = ((), (), s32[]{:S(2)}) async-start(), calls=%async_computation.12 | async-start | bytes 1572864 | tf_op jit(solution)/shard_map/reduce_scatter | solution.py:27
  629.3 86.2 %copy-start.21 = (f32[1024]{0:T(1024)S(1)}, f32[1024]{0:T(1024)}, u32[]{:S(2)}) copy-start(f32[1024]{0:T(1024)} %param.31) | copy-start | bytes 12292
  635.7 159.3 %copy-start.22 = (f32[1024]{0:T(1024)S(1)}, f32[1024]{0:T(1024)}, u32[]{:S(2)}) copy-start(f32[1024]{0:T(1024)} %param.33) | copy-start | bytes 12292
  721.9 150.0 %copy-start.23 = (f32[1024]{0:T(1024)S(1)}, f32[1024]{0:T(1024)}, u32[]{:S(2)}) copy-start(f32[1024]{0:T(1024)} %param.35) | copy-start | bytes 12292
  877.9 1.5 copy-start.8
  880.4 4.0 copy-start.3
  894.8 5.2 copy-start.9
  900.0 3.7 copy-start.12
  903.6 13.0 %copy-start.11 = (f32[2048]{0:T(1024)S(1)}, f32[2048]{0:T(1024)}, u32[]{:S(2)}) copy-start(f32[2048]{0:T(1024)} %param.23) | copy-start | bytes 24580
  903.7 25.4 %copy-start.18 = (f32[3072]{0:T(1024)S(1)}, f32[3072]{0:T(1024)}, u32[]{:S(2)}) copy-start(f32[3072]{0:T(1024)} %param.25) | copy-start | bytes 36868
  908.2 20.9 %all-gather.30.cloned.1.call-start = ((), (), s32[]{:S(2)}) async-start(), calls=%async_computation.13 | async-start | bytes 1572864 | tf_op jit(solution)/shard_map/all_gather | solution.py:22
  918.7 20.4 %copy-start.20 = (f32[3072]{0:T(1024)S(1)}, f32[3072]{0:T(1024)}, u32[]{:S(2)}) copy-start(f32[3072]{0:T(1024)} %param.27) | copy-start | bytes 36868
  918.7 47.2 %reduce-scatter.8.cloned.1.call-start = ((), (), s32[]{:S(2)}) async-start(), calls=%async_computation.14 | async-start | bytes 1572864 | tf_op jit(solution)/shard_map/reduce_scatter | solution.py:27
  929.1 10.0 %copy-start.16 = (bf16[256,2048]{1,0:T(8,128)(2,1)S(1)}, bf16[256,2048]{1,0:T(8,128)(2,1)}, u32[]{:S(2)}) copy-start(bf16[256,2048]{1,0:T(8,128)(2,1)} %all-gather.30.cloned.1.call-done) | copy-start | bytes 3145732
  939.1 26.8 %copy-start.1 = (bf16[128,2048]{1,0:T(8,128)(2,1)S(1)}, bf16[128,2048]{1,0:T(8,128)(2,1)}, u32[]{:S(2)}) copy-start(bf16[128,2048]{1,0:T(8,128)(2,1)} %reduce-scatter.6.cloned.1.call-done) | copy-start | bytes 1572868
Sparse Core Ops, SparseCore 0:
  10.1 11.7 all-gather.13
  24.6 152.6 all-gather.15
  180.1 149.5 all-gather.17
  332.2 193.6 all-gather.19
  543.2 6.5 reduce-scatter.3
  552.4 76.8 all-gather.31
  632.0 74.1 all-gather.25
  707.8 7.6 all-gather.21
  718.2 76.7 all-gather.27
  797.6 74.1 all-gather.23
  908.3 6.9 reduce-scatter.5
  918.8 10.2 all-gather.29
  956.3 9.5 reduce-scatter.7
